TPU v7x, 32 devices: a whole 2x2x4 slice. The times are simulated.
32 devices in a mesh: rep: 2 (over x), fs: 8 (over z, y), tp: 2 (over core).
Axes of the slice: x: 2, y: 2, z: 4, core: 2. Of those that a mesh axis runs over, the one named last changes fastest.
Arguments:
- tokens: bfloat16 [16, 192, 2048], P(('rep', 'fs'), 'tp'), may hold values from -6 to 6
- mix_gain: float32 [2048], replicated, may hold values from 0.1 to 1.9
- w_query: float32 [2048, 2048], P('fs', 'tp'), may hold values from -0.125 to 0.125
- w_key: float32 [2048, 2048], P('fs', 'tp'), may hold values from -0.125 to 0.125
- w_value: float32 [2048, 2048], P('fs', 'tp'), may hold values from -0.125 to 0.125
- w_out: float32 [2048, 2048], P('tp', 'fs'), may hold values from -0.125 to 0.125
- scale_query: float32 [2048], P('tp'), may hold values from 0.1 to 1.9
- scale_key: float32 [2048], P('tp'), may hold values from 0.1 to 1.9
- scale_value: float32 [2048], P('tp'), may hold values from 0.1 to 1.9
- scale_out: float32 [2048], replicated, may hold values from 0.1 to 1.9
- decay_rate: float32 [8], P('tp'), may hold values from 0.003 to 0.08
- mlp_gain: float32 [2048], replicated, may hold values from 0.1 to 1.9
- w_gate: float32 [2048, 3072], P('fs', 'tp'), may hold values from -0.125 to 0.125
- w_up: float32 [2048, 3072], P('fs', 'tp'), may hold values from -0.125 to 0.125
- w_down: float32 [3072, 2048], P('tp', 'fs'), may hold values from -0.109375 to 0.109375
- scale_gate: float32 [3072], P('tp'), may hold values from 0.1 to 1.9
- scale_up: float32 [3072], P('tp'), may hold values from 0.1 to 1.9
- scale_down: float32 [2048], replicated, may hold values from 0.1 to 1.9
Outputs:
- layer_out: bfloat16 [16, 192, 2048], P(('rep', 'fs'), 'tp')
All inputs are finite; a program needn't handle non-finite values.
Results may differ from a plain program's by a relative error of at most 0.015.
Values may be sent and summed in bfloat16 or wider, within the bound.
A program may use at most 64 MiB of HBM per device.

v0:
```python
import jax
import jax.numpy as jnp
from jax import lax
from jax.sharding import PartitionSpec as P

HEAD_DIM = 256
BLOCK = 64


EPS = 1e-06
ROPE_BASE = 10000.0


def rms_scale(values, gain):
    values = values.astype(jnp.float32)
    return values * lax.rsqrt(jnp.mean(values * values, axis=-1, keepdims=True) + EPS) * gain


def rotary(values, positions):
    width = values.shape[-1]
    half = width // 2
    inv_freq = 1.0 / ROPE_BASE ** (jnp.arange(0, width, 2, dtype=jnp.float32) / width)
    angles = positions.astype(jnp.float32)[:, None] * inv_freq[None, :]
    cosine = jnp.cos(angles)[:, None, :]
    sine = jnp.sin(angles)[:, None, :]
    first = values[..., :half]
    second = values[..., half:]
    return jnp.concatenate(
        [first * cosine - second * sine, first * sine + second * cosine], axis=-1
    )


def retention(query, keyed, valued, rates):
    length, heads, width = query.shape
    nblocks = length // BLOCK

    def split(values):
        return values.reshape(nblocks, BLOCK, heads, width).transpose(0, 2, 1, 3)

    log_gamma = -rates
    inside = jnp.arange(BLOCK, dtype=jnp.float32)
    distance = inside[:, None] - inside[None, :]
    inner_product = jnp.where(
        distance[None] >= 0.0,
        jnp.exp(log_gamma[:, None, None] * jnp.maximum(distance, 0.0)[None]),
        0.0,
    )
    query_decay = jnp.exp(log_gamma[:, None] * (inside[None, :] + 1.0))
    key_decay_factor = jnp.exp(log_gamma[:, None] * (BLOCK - 1.0 - inside[None, :]))
    block_decay = jnp.exp(log_gamma * BLOCK)

    def advance(state, blocks):
        query_block_tile, key_block_tile, value_block_tile = blocks
        attention_scores = jnp.einsum(
            "frk,fvk->frv", query_block_tile, key_block_tile, preferred_element_type=jnp.float32
        )
        decay_weights = (attention_scores * inner_product).astype(jnp.bfloat16)
        local = jnp.einsum(
            "hnm,hmv->hnv", decay_weights, value_block_tile, preferred_element_type=jnp.float32
        )
        carried = jnp.einsum(
            "hnd,hdv->hnv",
            query_block_tile.astype(jnp.float32) * query_decay[:, :, None],
            state,
            precision=lax.Precision.HIGHEST,
        )
        state_update = jnp.einsum(
            "asf,asp->afp",
            key_block_tile.astype(jnp.float32) * key_decay_factor[:, :, None],
            value_block_tile.astype(jnp.float32),
            precision=lax.Precision.HIGHEST,
        )
        return (state * block_decay[:, None, None] + state_update, local + carried)

    initial = jnp.zeros((heads, width, width), jnp.float32)
    _, outs = lax.scan(advance, initial, (split(query), split(keyed), split(valued)))
    return outs.transpose(0, 2, 1, 3).reshape(length, heads, width)


def per_device(
    tokens,
    mix_gain,
    w_query,
    w_key,
    w_value,
    w_out,
    scale_query,
    scale_key,
    scale_value,
    scale_out,
    decay_rate,
    mlp_gain,
    w_gate,
    w_up,
    w_down,
    scale_gate,
    scale_up,
    scale_down,
):
    own_rows = tokens[0]
    all_rows = lax.all_gather(own_rows, "tp", axis=0, tiled=True)
    gathered = rms_scale(all_rows, mix_gain).astype(jnp.bfloat16)
    length = gathered.shape[0]
    width = w_query.shape[1]
    shards = (
        lax.all_gather(w_query.astype(jnp.bfloat16), "fs", axis=0, tiled=True),
        lax.all_gather(w_key.astype(jnp.bfloat16), "fs", axis=0, tiled=True),
        lax.all_gather(w_value.astype(jnp.bfloat16), "fs", axis=0, tiled=True),
    )
    columns = gathered
    query_raw, key_raw, value_raw = tuple(
        (jnp.dot(columns, shard, preferred_element_type=jnp.float32) for shard in shards)
    )
    positions = jnp.arange(length)
    heads_here = width // HEAD_DIM
    query_rows = rotary(
        (query_raw * scale_query).reshape(length, heads_here, HEAD_DIM), positions
    ).astype(jnp.bfloat16)
    key_rows = rotary(
        (key_raw * scale_key).reshape(length, heads_here, HEAD_DIM), positions
    ).astype(jnp.bfloat16)
    value_rows = (
        (value_raw * scale_value).reshape(length, heads_here, HEAD_DIM).astype(jnp.bfloat16)
    )
    retained = retention(query_rows, key_rows, value_rows, decay_rate)
    attended = rms_scale(retained, 1.0).astype(jnp.bfloat16).reshape(length, width)
    out_whole = lax.all_gather(w_out.astype(jnp.bfloat16), "fs", axis=1, tiled=True)
    picked = attended
    mixed = lax.psum_scatter(
        (jnp.dot(picked, out_whole, preferred_element_type=jnp.float32) * scale_out).astype(
            jnp.bfloat16
        ),
        "tp",
        scatter_dimension=0,
        tiled=True,
    ).astype(jnp.float32)
    hidden_state = (own_rows.astype(jnp.float32) + mixed).astype(jnp.bfloat16)
    mlp_in = rms_scale(hidden_state, mlp_gain).astype(jnp.bfloat16)
    mlp_rows_in = lax.all_gather(mlp_in, "tp", axis=0, tiled=True)
    shards = (
        lax.all_gather(w_gate.astype(jnp.bfloat16), "fs", axis=0, tiled=True),
        lax.all_gather(w_up.astype(jnp.bfloat16), "fs", axis=0, tiled=True),
    )
    columns = mlp_rows_in
    gate_val, up_val = tuple(
        (jnp.dot(columns, shard, preferred_element_type=jnp.float32) for shard in shards)
    )
    down_whole = lax.all_gather(w_down.astype(jnp.bfloat16), "fs", axis=1, tiled=True)
    inner_product = (jax.nn.silu(gate_val * scale_gate) * (up_val * scale_up)).astype(jnp.bfloat16)
    picked = inner_product
    channel = lax.psum_scatter(
        (jnp.dot(picked, down_whole, preferred_element_type=jnp.float32) * scale_down).astype(
            jnp.bfloat16
        ),
        "tp",
        scatter_dimension=0,
        tiled=True,
    ).astype(jnp.float32)
    return (hidden_state.astype(jnp.float32) + channel).astype(jnp.bfloat16)[None]


def solution(mesh):
    in_specs = (
        P(("rep", "fs"), "tp", None),
        P(),
        P("fs", "tp"),
        P("fs", "tp"),
        P("fs", "tp"),
        P("tp", "fs"),
        P("tp"),
        P("tp"),
        P("tp"),
        P(),
        P("tp"),
        P(),
        P("fs", "tp"),
        P("fs", "tp"),
        P("tp", "fs"),
        P("tp"),
        P("tp"),
        P(),
    )
    out_specs = P(("rep", "fs"), "tp", None)
    return jax.shard_map(
        per_device, mesh=mesh, in_specs=in_specs, out_specs=out_specs, check_vma=False
    )
```

profile of v0, /device:TPU:0, one launch (start us, length us, event | category | flops | bytes accessed | tf_op | source)
XLA Modules:
  0.0 641.8 jit_solution(169841490198912978)
XLA Ops:
  6.5 2.2 convert_element_type.108
  8.8 0.0 all-gather.13.cloned.1.call-start
  8.8 0.9 convert_element_type.113
  9.7 0.0 all-gather.11.cloned.1.call-start
  9.8 0.4 copy-done.7
  10.1 0.9 convert_element_type.110
  11.1 0.0 all-gather.15.cloned.1.call-start
  11.1 0.8 convert_element_type.115
  12.0 0.0 reduce-scatter.3.cloned.1.call-start
  12.2 2.5 all-gather
  14.7 0.2 fusion.52
  14.9 0.4 multiply_cosine_fusion
  15.3 69.7 %all-gather.9.cloned.1.call-done = bf16[2048,1024]{1,0:T(8,128)(2,1)} async-done(((bf16[256,1024]{1,0:T(8,128)(2,1)}), bf16[2048,1024]{1,0:T(8,128)(2,1)}) %all-gather.9.cloned.1.call-update) | async-done | bytes 4194320 | tf_op jit(solution)/shard_map/all_gather | solution.py:107
  85.0 4.1 convolution_multiply_fusion.7
  89.2 1.5 reshape.164
  90.7 67.8 %all-gather.13.cloned.1.call-done = bf16[2048,1024]{1,0:T(8,128)(2,1)} async-done(((bf16[256,1024]{1,0:T(8,128)(2,1)}), bf16[2048,1024]{1,0:T(8,128)(2,1)}) %all-gather.13.cloned.1.call-update) | async-done | bytes 4194320 | tf_op jit(solution)/shard_map/all_gather | solution.py:106
  158.5 4.1 convolution_multiply_fusion.5
  162.6 2.4 reshape.165
  165.1 66.9 %all-gather.11.cloned.1.call-done = bf16[2048,1024]{1,0:T(8,128)(2,1)} async-done(((bf16[256,1024]{1,0:T(8,128)(2,1)}), bf16[2048,1024]{1,0:T(8,128)(2,1)}) %all-gather.11.cloned.1.call-update) | async-done | bytes 4194320 | tf_op jit(solution)/shard_map/all_gather | solution.py:108
  232.0 4.0 fusion.55
  236.0 1.3 convert_element_type.112
  237.3 1.3 fusion.70
  238.6 0.2 subtract_convert_fusion
  238.8 0.1 maximum_bitcast_fusion.1
  238.9 0.1 maximum_bitcast_fusion
  238.9 8.3 %while.15 = (s32[]{:T(128)}, f32[4,256,256]{2,1,0:T(8,128)S(1)}, f32[3,4,64,256]{3,2,1,0:T(8,128)}, f32[4]{0:T(128)S(1)}, bf16[3,4,64,256]{3,2,0,1:T(8,128)(2,1)...) while((s32[]{:T(128)}, f32[4,256,256]{2,1,0:T(8,128)S(1)}, ...), condition=%wide.region_2.3_spmd.clone.clone.clone, body=%wide.region_1.2_spmd.clone.clone.clone.sunk | while | flops 420872704 | bytes 4770468 | solution.py:76
  238.9 0.1 multiply_exponential_fusion.4
  239.0 0.8 fusion.98
  239.8 1.0 fusion.99
  240.8 0.8 convolution_add_fusion.3
  241.7 0.1 multiply_exponential_fusion.4
  241.8 0.8 fusion.98
  242.6 1.0 fusion.99
  243.6 0.8 convolution_add_fusion.3
  244.5 0.1 multiply_exponential_fusion.4
  244.5 0.8 fusion.98
  245.4 1.0 fusion.99
  246.4 0.8 convolution_add_fusion.3
  247.2 1.4 multiply_reduce_fusion
  248.6 0.1 copy.46
  248.8 0.3 mul.353
  249.0 0.1 copy.55
  249.2 0.5 copy.43
  249.7 0.1 copy.54
  249.9 57.2 %all-gather.15.cloned.1.call-done = bf16[1024,2048]{1,0:T(8,128)(2,1)} async-done(((bf16[1024,256]{1,0:T(8,128)(2,1)}), bf16[1024,2048]{1,0:T(8,128)(2,1)}) %all-gather.15.cloned.1.call-update) | async-done | bytes 4194320 | tf_op jit(solution)/shard_map/all_gather | solution.py:127
  307.1 4.2 fusion.49
  311.3 0.0 all-gather.17.cloned.1.call-start
  311.4 1.0 convert_element_type.121
  312.4 0.0 all-gather.19.cloned.1.call-start
  312.4 0.6 copy-done.4
  313.0 1.0 convert_element_type.122
  314.0 0.0 all-gather.21.cloned.1.call-start
  314.1 1.0 convert_element_type.124
  315.2 2.6 reduce-scatter.3.cloned.1.call-done
  317.8 1.2 fusion.56
  319.0 1.2 fusion.58
  320.2 2.5 all_gather.32
  322.8 96.9 %all-gather.17.cloned.1.call-done = bf16[2048,1536]{1,0:T(8,128)(2,1)} async-done(((bf16[256,1536]{1,0:T(8,128)(2,1)}), bf16[2048,1536]{1,0:T(8,128)(2,1)}) %all-gather.17.cloned.1.call-update) | async-done | bytes 6291472 | tf_op jit(solution)/shard_map/all_gather | solution.py:141
  419.7 4.2 convolution_multiply_fusion.2
  423.9 94.9 %all-gather.19.cloned.1.call-done = bf16[2048,1536]{1,0:T(8,128)(2,1)} async-done(((bf16[256,1536]{1,0:T(8,128)(2,1)}), bf16[2048,1536]{1,0:T(8,128)(2,1)}) %all-gather.19.cloned.1.call-update) | async-done | bytes 6291472 | tf_op jit(solution)/shard_map/all_gather | solution.py:142
  518.8 99.7 %all-gather.21.cloned.1.call-done = bf16[1536,2048]{1,0:T(8,128)(2,1)} async-done(((bf16[1536,256]{1,0:T(8,128)(2,1)}), bf16[1536,2048]{1,0:T(8,128)(2,1)}) %all-gather.21.cloned.1.call-update) | async-done | bytes 6291472 | tf_op jit(solution)/shard_map/all_gather | solution.py:148
  618.6 8.3 %fusion.50 = bf16[192,2048]{1,0:T(8,128)(2,1)} fusion(bf16[1536,2048]{1,0:T(8,128)(2,1)} %all-gather.21.cloned.1.call-done, f32[2048]{0:T(1024)S(1)} %copy-done.13, bf16[192,2048]{1,0:T(8,128)(2,1)S(1)} %all_gather.32, bf16[2048,1536]{1,0:T(8,128)(2,1)} %all-gather.19.cloned.1.call-done, f32[192,1536]{1,0:T(8,128)S(1)} %convolution_multiply_fusion.2, ...), kind=kOutput, calls=%fused_computation.51 | convolution fusion | flops 2418769920 | bytes 15349760 | tf_op jit(solution)/shard_map/dot_general | solution.py:152
  626.9 6.5 %reduce-scatter.5.cloned.1.call-done = bf16[96,2048]{1,0:T(8,128)(2,1)} async-done(((bf16[192,2048]{1,0:T(8,128)(2,1)}), bf16[96,2048]{1,0:T(8,128)(2,1)}) %reduce-scatter.5.cloned.1.call-update) | async-done | bytes 393232 | tf_op jit(solution)/shard_map/reduce_scatter | solution.py:151
  633.4 1.9 fusion.63
  (59 shorter events, 0.4 us)
Async XLA Ops:
  6.5 2.3 copy-start.6
  6.5 78.5 %all-gather.9.cloned.1.call-start = ((), (), s32[]{:S(2)}) async-start(), calls=%async_computation.2 | async-start | bytes 4718592 | tf_op jit(solution)/shard_map/all_gather | solution.py:107
  8.7 1.4 copy-start.7
  8.8 149.7 %all-gather.13.cloned.1.call-start = ((), (), s32[]{:S(2)}) async-start(), calls=%async_computation.4 | async-start | bytes 4718592 | tf_op jit(solution)/shard_map/all_gather | solution.py:106
  9.7 1.4 copy-start.8
  9.7 222.3 %all-gather.11.cloned.1.call-start = ((), (), s32[]{:S(2)}) async-start(), calls=%async_computation.3 | async-start | bytes 4718592 | tf_op jit(solution)/shard_map/all_gather | solution.py:108
  11.0 1.1 copy-start
  11.1 296.0 %all-gather.15.cloned.1.call-start = ((), (), s32[]{:S(2)}) async-start(), calls=%async_computation.5 | async-start | bytes 4718592 | tf_op jit(solution)/shard_map/all_gather | solution.py:127
  12.0 2.9 copy-start.18
  12.0 73.0 %copy-start.11 = (f32[2048]{0:T(1024)S(1)}, f32[2048]{0:T(1024)}, u32[]{:S(2)}) copy-start(f32[2048]{0:T(1024)} %param.21) | copy-start | bytes 24580
  12.0 73.0 %copy-start.15 = (f32[1024]{0:T(1024)S(1)}, f32[1024]{0:T(1024)}, u32[]{:S(2)}) copy-start(f32[1024]{0:T(1024)} %param.27) | copy-start | bytes 12292
  12.0 305.8 %reduce-scatter.3.cloned.1.call-start = ((), (), s32[]{:S(2)}) async-start(), calls=%async_computation.6 | async-start | bytes 1179648 | tf_op jit(solution)/shard_map/reduce_scatter | solution.py:129
  89.2 69.3 %copy-start.16 = (f32[1024]{0:T(1024)S(1)}, f32[1024]{0:T(1024)}, u32[]{:S(2)}) copy-start(f32[1024]{0:T(1024)} %param.26) | copy-start | bytes 12292
  162.6 69.3 %copy-start.17 = (f32[1024]{0:T(1024)S(1)}, f32[1024]{0:T(1024)}, u32[]{:S(2)}) copy-start(f32[1024]{0:T(1024)} %param.28) | copy-start | bytes 12292
  247.2 2.0 copy-start.2
  249.2 57.9 %copy-start.9 = (f32[2048]{0:T(1024)S(1)}, f32[2048]{0:T(1024)}, u32[]{:S(2)}) copy-start(f32[2048]{0:T(1024)} %param.29) | copy-start | bytes 24580
  307.1 4.3 copy-start.3
  311.3 1.7 copy-start.4
  311.3 108.4 %all-gather.17.cloned.1.call-start = ((), (), s32[]{:S(2)}) async-start(), calls=%async_computation.7 | async-start | bytes 7077888 | tf_op jit(solution)/shard_map/all_gather | solution.py:141
  312.4 1.7 copy-start.5
  312.4 206.4 %all-gather.19.cloned.1.call-start = ((), (), s32[]{:S(2)}) async-start(), calls=%async_computation.8 | async-start | bytes 7077888 | tf_op jit(solution)/shard_map/all_gather | solution.py:142
  314.0 5.0 copy-start.10
  314.0 304.5 %all-gather.21.cloned.1.call-start = ((), (), s32[]{:S(2)}) async-start(), calls=%async_computation.9 | async-start | bytes 7077888 | tf_op jit(solution)/shard_map/all_gather | solution.py:148
  315.1 104.6 %copy-start.12 = (f32[1536]{0:T(1024)S(1)}, f32[1536]{0:T(1024)}, u32[]{:S(2)}) copy-start(f32[1536]{0:T(1024)} %param.35) | copy-start | bytes 18436
  315.1 318.2 %reduce-scatter.5.cloned.1.call-start = ((), (), s32[]{:S(2)}) async-start(), calls=%async_computation.10 | async-start | bytes 1179648 | tf_op jit(solution)/shard_map/reduce_scatter | solution.py:151
  322.8 295.8 %copy-start.13 = (f32[2048]{0:T(1024)S(1)}, f32[2048]{0:T(1024)}, u32[]{:S(2)}) copy-start(f32[2048]{0:T(1024)} %param.37) | copy-start | bytes 24580
  322.8 295.8 %copy-start.14 = (f32[1536]{0:T(1024)S(1)}, f32[1536]{0:T(1024)}, u32[]{:S(2)}) copy-start(f32[1536]{0:T(1024)} %param.36) | copy-start | bytes 18436
  423.9 209.5 %copy-start.1 = (bf16[96,2048]{1,0:T(8,128)(2,1)S(1)}, bf16[96,2048]{1,0:T(8,128)(2,1)}, u32[]{:S(2)}) copy-start(bf16[96,2048]{1,0:T(8,128)(2,1)} %reduce-scatter.3.cloned.1.call-done) | copy-start | bytes 1179652
Sparse Core Ops, SparseCore 0:
  9.5 75.5 all-gather.8
  87.1 71.3 all-gather.12
  160.6 71.3 all-gather.10
  233.9 73.1 all-gather.14
  311.4 6.3 reduce-scatter.2
  319.8 99.8 all-gather.16
  421.9 96.9 all-gather.18
  520.9 97.6 all-gather.20
  627.0 6.3 reduce-scatter.4
where the time goes:
time: 642 us
  waiting for transfers between devices  563 us (88%)
  matrix products  36.9 us (6%)
  other arithmetic  14.7 us (2%)
  between operations  13.5 us (2%)
  local copies, waits for them, and re-layouts  8.76 us (1%)
    all_gather x1, waiting for transfers between devices, per_device(): lax.all_gather(w_down.astype(jnp.bfloat16), 'fs', axis=1, tiled=True)  99.7 us
    all_gather x1, waiting for transfers between devices, per_device(): lax.all_gather(w_gate.astype(jnp.bfloat16), 'fs', axis=0, tiled=True)  96.9 us
    all_gather x1, waiting for transfers between devices, per_device(): lax.all_gather(w_up.astype(jnp.bfloat16), 'fs', axis=0, tiled=True)  94.9 us
    all_gather x1, waiting for transfers between devices, per_device(): lax.all_gather(w_key.astype(jnp.bfloat16), 'fs', axis=0, tiled=True)  69.7 us
    all_gather x1, waiting for transfers between devices, per_device(): lax.all_gather(w_query.astype(jnp.bfloat16), 'fs', axis=0, tiled=True)  67.8 us
    all_gather x1, waiting for transfers between devices, per_device(): lax.all_gather(w_value.astype(jnp.bfloat16), 'fs', axis=0, tiled=True)  66.9 us
    all_gather x1, waiting for transfers between devices, per_device(): lax.all_gather(w_out.astype(jnp.bfloat16), 'fs', axis=1, tiled=True)  57.2 us
    dot_general x4, matrix products, per_device(): jnp.dot(columns, shard, preferred_element_type=jnp.float32)  16.4 us
  transfers between devices with their start and end apart: 9, of which 9 were waited for; matrix products, arithmetic and copies ran while one was open for 7% of the time, Pallas kernels for 0%

commit v1 on v0

v1 whole, which is shorter than its diff:
```python
import functools

import jax
import jax.numpy as jnp
from jax import lax
from jax.sharding import PartitionSpec as P

HEAD_DIM = 256

EPS = 1e-06
ROPE_BASE = 10000.0


def rms_scale(values, gain):
    values = values.astype(jnp.float32)
    return values * lax.rsqrt(jnp.mean(values * values, axis=-1, keepdims=True) + EPS) * gain


def rotary(values, positions):
    width = values.shape[-1]
    half = width // 2
    inv_freq = 1.0 / ROPE_BASE ** (jnp.arange(0, width, 2, dtype=jnp.float32) / width)
    angles = positions.astype(jnp.float32)[:, None] * inv_freq[None, :]
    cosine = jnp.cos(angles)[:, None, :]
    sine = jnp.sin(angles)[:, None, :]
    first = values[..., :half]
    second = values[..., half:]
    return jnp.concatenate(
        [first * cosine - second * sine, first * sine + second * cosine], axis=-1
    )


def retention(query, keyed, valued, rates):
    length = query.shape[1]
    place = jnp.arange(length, dtype=jnp.float32)
    distance = place[:, None] - place[None, :]
    decay = jnp.where(
        distance[None] >= 0.0,
        jnp.exp(-rates[:, None, None] * jnp.maximum(distance, 0.0)[None]),
        0.0,
    )
    scores = jnp.einsum("bnhd,bmhd->bhnm", query, keyed, preferred_element_type=jnp.float32)
    weights = (scores * decay[None]).astype(jnp.bfloat16)
    return jnp.einsum("bhnm,bmhv->bnhv", weights, valued, preferred_element_type=jnp.float32)


def per_device(
    reps,
    shards,
    halves,
    tokens,
    mix_gain,
    w_query,
    w_key,
    w_value,
    w_out,
    scale_query,
    scale_key,
    scale_value,
    scale_out,
    decay_rate,
    mlp_gain,
    w_gate,
    w_up,
    w_down,
    scale_gate,
    scale_up,
    scale_down,
):
    heads_tp = w_query.shape[1] // HEAD_DIM
    xs = 2 if reps == 2 and heads_tp % 2 == 0 else 1
    ys = 2 if shards % 2 == 0 and (heads_tp // xs) % 2 == 0 else 1
    team = xs * ys
    x = lax.axis_index("rep") if xs > 1 else 0
    fs_index = lax.axis_index("fs")
    y = fs_index % ys
    me = x * ys + y
    own_half = lax.axis_index("tp")

    def flip_chip(values, dx, dy):
        perm = []
        for r in range(reps):
            for f in range(shards):
                target_r = (r ^ 1) if dx else r
                target_f = (f ^ 1) if dy else f
                perm.append((r * shards + f, target_r * shards + target_f))
        return lax.ppermute(values, ("rep", "fs"), perm)

    offsets = [(dx, dy) for dx in range(xs) for dy in range(ys)]

    def cut(values, index, axis):
        size = values.shape[axis] // team
        return lax.dynamic_slice_in_dim(values, index * size, size, axis)

    def share(index, columned, rowed):
        parts = [cut(w, index, 1).astype(jnp.bfloat16) for w in columned]
        parts += [cut(w, index, 0).astype(jnp.bfloat16).T for w in rowed]
        return jnp.concatenate(parts, axis=1)

    def gather(columned, rowed):
        mine = share(me, columned, rowed)
        if ys > 1:
            theirs = flip_chip(share(x * ys + (1 - y), columned, rowed), 0, 1)
            first = jnp.where(y == 0, mine, theirs)
            second = jnp.where(y == 0, theirs, mine)
            mine = jnp.concatenate([first, second], axis=0)
        groups = [[s * ys + c for s in range(shards // ys)] for c in range(ys)]
        return lax.all_gather(mine, "fs", axis=0, tiled=True, axis_index_groups=groups)

    def gather_rows(rows):
        stacked = jnp.stack([flip_chip(rows, dx, dy) if dx or dy else rows for dx, dy in offsets])
        pieces = lax.all_gather(stacked, "tp", axis=1, tiled=True)
        return pieces.reshape(-1, rows.shape[-1])

    def scatter_rows(partial, rows):
        split = partial.astype(jnp.bfloat16).reshape(team, halves * rows, -1)
        if halves == 2:
            keep = lax.dynamic_slice_in_dim(split, own_half * rows, rows, 1)
            give = lax.dynamic_slice_in_dim(split, (1 - own_half) * rows, rows, 1)
            got = lax.ppermute(give, "tp", [(0, 1), (1, 0)])
            summed = keep.astype(jnp.float32) + got.astype(jnp.float32)
        else:
            summed = lax.psum_scatter(split, "tp", scatter_dimension=1, tiled=True)
            summed = summed.astype(jnp.float32)
        total = summed[0]
        for index, (dx, dy) in enumerate(offsets):
            if dx or dy:
                sent = flip_chip(summed[index].astype(jnp.bfloat16), dx, dy)
                total = total + sent.astype(jnp.float32)
        return total

    own_rows = tokens[0]
    rows = own_rows.shape[0]
    length = rows * halves
    normed = gather_rows(rms_scale(own_rows, mix_gain).astype(jnp.bfloat16))
    mixer = gather((w_query, w_key, w_value), (w_out,))
    width = w_query.shape[1] // team
    heads_here = width // HEAD_DIM
    raw = jnp.dot(normed, mixer[:, : 3 * width], preferred_element_type=jnp.float32)
    positions = jnp.arange(length)

    def heads_of(index, scale):
        values = raw[:, index * width : (index + 1) * width] * cut(scale, me, 0)
        return values.reshape(team, length, heads_here, HEAD_DIM)

    query = rotary(heads_of(0, scale_query), positions).astype(jnp.bfloat16)
    keyed = rotary(heads_of(1, scale_key), positions).astype(jnp.bfloat16)
    valued = heads_of(2, scale_value).astype(jnp.bfloat16)
    retained = retention(query, keyed, valued, cut(decay_rate, me, 0))
    attended = rms_scale(retained, 1.0).astype(jnp.bfloat16).reshape(team * length, width)
    contract = (((1,), (1,)), ((), ()))
    partial = (
        lax.dot_general(
            attended, mixer[:, 3 * width :], contract, preferred_element_type=jnp.float32
        )
        * scale_out
    )
    mixed = scatter_rows(partial, rows)
    hidden_state = (own_rows.astype(jnp.float32) + mixed).astype(jnp.bfloat16)
    mlp_in = gather_rows(rms_scale(hidden_state, mlp_gain).astype(jnp.bfloat16))
    channel_mixer = gather((w_gate, w_up), (w_down,))
    units = w_gate.shape[1] // team
    both = jnp.dot(mlp_in, channel_mixer[:, : 2 * units], preferred_element_type=jnp.float32)
    gate_val = both[:, :units] * cut(scale_gate, me, 0)
    up_val = both[:, units:] * cut(scale_up, me, 0)
    inner = (jax.nn.silu(gate_val) * up_val).astype(jnp.bfloat16)
    partial = (
        lax.dot_general(
            inner, channel_mixer[:, 2 * units :], contract, preferred_element_type=jnp.float32
        )
        * scale_down
    )
    channel = scatter_rows(partial, rows)
    return (hidden_state.astype(jnp.float32) + channel).astype(jnp.bfloat16)[None]


def solution(mesh):
    in_specs = (
        P(("rep", "fs"), "tp", None),
        P(),
        P("fs", "tp"),
        P("fs", "tp"),
        P("fs", "tp"),
        P("tp", "fs"),
        P("tp"),
        P("tp"),
        P("tp"),
        P(),
        P("tp"),
        P(),
        P("fs", "tp"),
        P("fs", "tp"),
        P("tp", "fs"),
        P("tp"),
        P("tp"),
        P(),
    )
    out_specs = P(("rep", "fs"), "tp", None)
    body = functools.partial(
        per_device, mesh.shape["rep"], mesh.shape["fs"], mesh.shape["tp"]
    )
    return jax.shard_map(
        body, mesh=mesh, in_specs=in_specs, out_specs=out_specs, check_vma=False
    )
```

time: 642 us -> 275 us (0.43)
  waiting for transfers between devices: 563 us -> 197 us
  matrix products: 36.9 us -> 17.1 us
  starting transfers between devices: 0.34 us -> 19 us
    all_gather x7 -> x4, waiting for transfers between devices: 553 us -> 105 us  [the longest x2 93 us: gather(): lax.all_gather(mine, 'fs', axis=0, tiled=True, axis_index_groups=groups)]
    ppermute x0 -> x16, waiting for transfers between devices: none -> 92.3 us  [the longest x14 85.4 us: flip_chip(): return lax.ppermute(values, ('rep', 'fs'), perm)]
    dot_general x15 -> x5, matrix products: 36.9 us -> 17.1 us  [the longest x1 5.49 us: per_device(): jnp.dot(mlp_in, channel_mixer[:, :2 * units], preferred_element_type=jnp....]
    ppermute x0 -> x16, starting transfers between devices: none -> 18.7 us  [the longest x14 18.4 us: flip_chip(): return lax.ppermute(values, ('rep', 'fs'), perm)]
    reduce_scatter x2 -> x0, waiting for transfers between devices: 9.14 us -> none  [the longest x1 6.5 us: per_device(): lax.psum_scatter((jnp.dot(picked, down_whole, preferred_element_type=jnp....]
    dynamic_slice x0 -> x10, local copies, waits for them, and re-layouts: none -> 8.56 us  [the longest x8 7.11 us: cut(): return lax.dynamic_slice_in_dim(values, index * size, size, axis)]
  transfers between devices with their start and end apart: 9 -> 20, of which waited for: 9 -> 19; matrix products, arithmetic and copies ran while one was open for 7% -> 11% of each run, Pallas kernels for 0% -> 0%
where the time goes in v1:
time: 275 us
  waiting for transfers between devices  197 us (72%)
  starting transfers between devices  19 us (7%)
  matrix products  17.1 us (6%)
  other arithmetic  14.6 us (5%)
  between operations  14.2 us (5%)
  local copies, waits for them, and re-layouts  12.3 us (4%)
    all_gather x2, waiting for transfers between devices, gather(): lax.all_gather(mine, 'fs', axis=0, tiled=True, axis_index_groups=groups)  93 us
    ppermute x14, waiting for transfers between devices, flip_chip(): return lax.ppermute(values, ('rep', 'fs'), perm)  85.4 us
    ppermute x14, starting transfers between devices, flip_chip(): return lax.ppermute(values, ('rep', 'fs'), perm)  18.4 us
    all_gather x2, waiting for transfers between devices, gather_rows(): pieces = lax.all_gather(stacked, 'tp', axis=1, tiled=True)  12 us
    dynamic_slice x8, local copies, waits for them, and re-layouts, cut(): return lax.dynamic_slice_in_dim(values, index * size, size, axis)  7.11 us
    ppermute x2, waiting for transfers between devices, scatter_rows(): got = lax.ppermute(give, 'tp', [(0, 1), (1, 0)])  6.94 us
  transfers between devices with their start and end apart: 20, of which 19 were waited for; matrix products, arithmetic and copies ran while one was open for 11% of the time, Pallas kernels for 0%

profile of v1, /device:TPU:0, one launch (start us, length us, event | category | flops | bytes accessed | tf_op | source)
XLA Modules:
  0.0 274.6 jit_solution(17315387092472695725)
XLA Ops:
  6.5 1.2 fusion.12
  7.7 1.2 fusion.14
  8.9 3.1 %collective-permute-start = (bf16[96,2048]{1,0:T(8,128)(2,1)S(1)}, bf16[96,2048]{1,0:T(8,128)(2,1)S(1)}, u32[]{:S(2)}, u32[]{:S(2)}) collective-permute-start(bf16[96,2048]{1,0:T(8,128)(2,1)S(1)} %fusion.14), channel_id=1, source_target_pairs={{0,2},{2,0},{4,6},{6,4},{8,10},{10,8},{12,14},{14,12},{16,18},{18,... | collective-permute-start | bytes 1179656 | tf_op jit(solution)/shard_map/ppermute | solution.py:87
  12.0 1.5 collective-permute-start.1
  13.5 1.2 fusion.17
  14.7 6.4 %collective-permute-done = bf16[96,2048]{1,0:T(8,128)(2,1)S(1)} collective-permute-done((bf16[96,2048]{1,0:T(8,128)(2,1)S(1)}, bf16[96,2048]{1,0:T(8,128)(2,1)S(1)}, u32[]{:S(2)}, u32[]{:S(2)}) %collective-permute-start) | collective-permute-done | bytes 393248 | tf_op jit(solution)/shard_map/ppermute | solution.py:87
  21.1 2.9 %collective-permute-done.1 = bf16[96,2048]{1,0:T(8,128)(2,1)S(1)} collective-permute-done((bf16[96,2048]{1,0:T(8,128)(2,1)S(1)}, bf16[96,2048]{1,0:T(8,128)(2,1)S(1)}, u32[]{:S(2)}, u32[]{:S(2)}) %collective-permute-start.1) | collective-permute-done | bytes 393248 | tf_op jit(solution)/shard_map/ppermute | solution.py:87
  23.9 6.8 %collective-permute-done.2 = bf16[96,2048]{1,0:T(8,128)(2,1)S(1)} collective-permute-done((bf16[96,2048]{1,0:T(8,128)(2,1)S(1)}, bf16[96,2048]{1,0:T(8,128)(2,1)S(1)}, u32[]{:S(2)}, u32[]{:S(2)}) %collective-permute-start.2) | collective-permute-done | bytes 393248 | tf_op jit(solution)/shard_map/ppermute | solution.py:87
  30.8 1.4 pad_maximum_fusion
  32.2 1.3 constant_dynamic-slice_fusion.10
  33.7 1.3 fusion.54
  35.1 1.7 collective-permute-start.3
  37.2 10.8 %collective-permute-done.3 = bf16[256,1024]{0,1:T(8,128)(2,1)S(1)} collective-permute-done((bf16[256,1024]{0,1:T(8,128)(2,1)S(1)}, bf16[256,1024]{0,1:T(8,128)(2,1)S(1)}, u32[]{:S(2)}, u32[]{:S(2)}) %collective-permute-start.3) | collective-permute-done | bytes 524320 | tf_op jit(solution)/shard_map/ppermute | solution.py:87
  48.2 1.1 pad_maximum_fusion.3
  49.4 1.5 constant_dynamic-slice_fusion.3
  51.1 1.2 fusion.51
  52.3 1.5 collective-permute-start.11
  53.8 0.8 dynamic_slice.80
  54.6 0.8 dynamic_slice.81
  55.3 0.8 dynamic_slice.82
  56.1 0.6 dynamic_slice.83
  57.7 0.4 multiply_cosine_fusion
  58.2 7.6 %collective-permute-done.11 = bf16[256,1152]{0,1:T(8,128)(2,1)S(1)} collective-permute-done((bf16[256,1152]{0,1:T(8,128)(2,1)S(1)}, bf16[256,1152]{0,1:T(8,128)(2,1)S(1)}, u32[]{:S(2)}, u32[]{:S(2)}) %collective-permute-start.11) | collective-permute-done | bytes 589856 | tf_op jit(solution)/shard_map/ppermute | solution.py:87
  65.8 0.2 broadcast_select_fusion.1
  66.0 1.1 pad_maximum_fusion.2
  67.1 0.2 all-gather.9.cloned.1.call-start
  67.4 63.9 %all-gather.7.cloned.1.call-done = bf16[2048,1024]{0,1:T(8,128)(2,1)} async-done(((bf16[512,1024]{0,1:T(8,128)(2,1)}), bf16[2048,1024]{0,1:T(8,128)(2,1)}) %all-gather.7.cloned.1.call-update) | async-done | bytes 4194320 | tf_op jit(solution)/shard_map/all_gather | solution.py:108
  131.3 5.5 %fusion.2 = f32[768,768]{1,0:T(8,128)S(1)} fusion(bf16[768,2048]{1,0:T(8,128)(2,1)} %bitcast.109, bf16[2048,1024]{0,1:T(8,128)(2,1)} %all-gather.7.cloned.1.call-done), kind=kOutput, calls=%fused_computation.4 | convolution fusion | flops 2415919104 | bytes 8650752 | tf_op jit(solution)/shard_map/dot_general | solution.py:139
  137.0 0.2 fusion.49
  137.2 0.5 multiply_reduce_fusion
  138.0 2.3 multiply_convert_fusion.1
  140.3 1.3 constant_dynamic-slice_fusion.5
  141.6 3.7 %collective-permute-done.4 = bf16[4,96,2048]{2,1,0:T(8,128)(2,1)} collective-permute-done((bf16[4,96,2048]{2,1,0:T(8,128)(2,1)}, bf16[4,96,2048]{2,1,0:T(8,128)(2,1)}, u32[]{:S(2)}, u32[]{:S(2)}) %collective-permute-start.4) | collective-permute-done | bytes 1572896 | tf_op jit(solution)/shard_map/ppermute | solution.py:120
  145.4 2.0 fusion.61
  147.5 1.6 collective-permute-start.5
  149.1 1.5 collective-permute-start.6
  150.6 0.5 collective-permute-start.7
  151.1 7.7 %collective-permute-done.5 = bf16[96,2048]{1,0:T(8,128)(2,1)S(1)} collective-permute-done((bf16[96,2048]{1,0:T(8,128)(2,1)S(1)}, bf16[96,2048]{1,0:T(8,128)(2,1)S(1)}, u32[]{:S(2)}, u32[]{:S(2)}) %collective-permute-start.5) | collective-permute-done | bytes 393248 | tf_op jit(solution)/shard_map/ppermute | solution.py:87
  158.8 2.4 collective-permute-done.6
  161.1 7.2 %collective-permute-done.7 = bf16[96,2048]{1,0:T(8,128)(2,1)S(1)} collective-permute-done((bf16[96,2048]{1,0:T(8,128)(2,1)S(1)}, bf16[96,2048]{1,0:T(8,128)(2,1)S(1)}, u32[]{:S(2)}, u32[]{:S(2)}) %collective-permute-start.7) | collective-permute-done | bytes 393248 | tf_op jit(solution)/shard_map/ppermute | solution.py:87
  168.4 0.4 fusion.18
  169.0 1.6 collective-permute-start.8
  170.6 1.5 collective-permute-start.9
  172.0 0.5 collective-permute-start.10
  172.7 7.4 %collective-permute-done.8 = bf16[96,2048]{1,0:T(8,128)(2,1)S(1)} collective-permute-done((bf16[96,2048]{1,0:T(8,128)(2,1)S(1)}, bf16[96,2048]{1,0:T(8,128)(2,1)S(1)}, u32[]{:S(2)}, u32[]{:S(2)}) %collective-permute-start.8) | collective-permute-done | bytes 393248 | tf_op jit(solution)/shard_map/ppermute | solution.py:87
  180.1 2.4 collective-permute-done.9
  182.5 6.2 %collective-permute-done.10 = bf16[96,2048]{1,0:T(8,128)(2,1)S(1)} collective-permute-done((bf16[96,2048]{1,0:T(8,128)(2,1)S(1)}, bf16[96,2048]{1,0:T(8,128)(2,1)S(1)}, u32[]{:S(2)}, u32[]{:S(2)}) %collective-permute-start.10) | collective-permute-done | bytes 393248 | tf_op jit(solution)/shard_map/ppermute | solution.py:87
  188.8 1.4 pad_maximum_fusion.1
  190.2 0.8 dynamic_slice.92
  191.0 0.8 dynamic_slice.93
  191.7 29.1 %all-gather.11.cloned.1.call-done = bf16[2048,1152]{0,1:T(8,128)(2,1)} async-done(((bf16[512,1152]{0,1:T(8,128)(2,1)}), bf16[2048,1152]{0,1:T(8,128)(2,1)}) %all-gather.11.cloned.1.call-update) | async-done | bytes 4718608 | tf_op jit(solution)/shard_map/all_gather | solution.py:108
  220.8 12.0 %all-gather.9.cloned.1.call-done = bf16[4,192,2048]{2,1,0:T(8,128)(2,1)} async-done(((bf16[4,96,2048]{2,1,0:T(8,128)(2,1)}), bf16[4,192,2048]{2,1,0:T(8,128)(2,1)}) %all-gather.9.cloned.1.call-update) | async-done | bytes 3145744 | tf_op jit(solution)/shard_map/all_gather | solution.py:112
  232.8 5.5 %fusion = f32[768,768]{1,0:T(8,128)S(1)} fusion(bf16[768,2048]{1,0:T(8,128)(2,1)} %bitcast.110, bf16[2048,1152]{0,1:T(8,128)(2,1)} %all-gather.11.cloned.1.call-done), kind=kOutput, calls=%fused_computation.2 | convolution fusion | flops 2415919104 | bytes 8650752 | tf_op jit(solution)/shard_map/dot_general | solution.py:163
  238.3 3.3 %multiply_convert_fusion = bf16[768,2048]{1,0:T(8,128)(2,1)S(1)} fusion(f32[2048]{0:T(1024)S(1)} %copy-done.3, bf16[2048,1152]{0,1:T(8,128)(2,1)} %all-gather.11.cloned.1.call-done, f32[768,768]{1,0:T(8,128)S(1)} %fusion, f32[384]{0:T(512)S(1)} %dynamic_slice.93, f32[384]{0:T(512)S(1)} %dynamic_slice.92), kind=kOutput, calls=%fused_computation | convolution fusion | flops 1213464576 | bytes 7089152 | tf_op jit(solution)/shard_map/dot_general | solution.py:168
  241.7 0.3 collective-permute-start.12
  242.0 3.2 %collective-permute-done.12 = bf16[4,96,2048]{2,1,0:T(8,128)(2,1)S(1)} collective-permute-done((bf16[4,96,2048]{2,1,0:T(8,128)(2,1)S(1)}, bf16[4,96,2048]{2,1,0:T(8,128)(2,1)S(1)}, u32[]{:S(2)}, u32[]{:S(2)}) %collective-permute-start.12) | collective-permute-done | bytes 1572896 | tf_op jit(solution)/shard_map/ppermute | solution.py:120
  245.2 0.7 fusion.59
  246.0 1.8 collective-permute-start.13
  247.8 1.5 collective-permute-start.14
  249.3 0.3 collective-permute-start.15
  249.6 7.8 %collective-permute-done.13 = bf16[96,2048]{1,0:T(8,128)(2,1)S(1)} collective-permute-done((bf16[96,2048]{1,0:T(8,128)(2,1)S(1)}, bf16[96,2048]{1,0:T(8,128)(2,1)S(1)}, u32[]{:S(2)}, u32[]{:S(2)}) %collective-permute-start.13) | collective-permute-done | bytes 393248 | tf_op jit(solution)/shard_map/ppermute | solution.py:87
  257.4 2.4 collective-permute-done.14
  259.8 7.2 %collective-permute-done.15 = bf16[96,2048]{1,0:T(8,128)(2,1)S(1)} collective-permute-done((bf16[96,2048]{1,0:T(8,128)(2,1)S(1)}, bf16[96,2048]{1,0:T(8,128)(2,1)S(1)}, u32[]{:S(2)}, u32[]{:S(2)}) %collective-permute-start.15) | collective-permute-done | bytes 393248 | tf_op jit(solution)/shard_map/ppermute | solution.py:87
  267.0 1.0 fusion.33
  (46 shorter events, 2.8 us)
Async XLA Ops:
  6.5 60.8 %all-gather.5.cloned.1.call-start = ((), (), s32[]{:S(2)}) async-start(), calls=%async_computation | async-start | bytes 4718592 | tf_op jit(solution)/shard_map/all_gather | solution.py:112
  8.9 12.2 %collective-permute-start = (bf16[96,2048]{1,0:T(8,128)(2,1)S(1)}, bf16[96,2048]{1,0:T(8,128)(2,1)S(1)}, u32[]{:S(2)}, u32[]{:S(2)}) collective-permute-start(bf16[96,2048]{1,0:T(8,128)(2,1)S(1)} %fusion.14), channel_id=1, source_target_pairs={{0,2},{2,0},{4,6},{6,4},{8,10},{10,8},{12,14},{14,12},{16,18},{18,... | collective-permute-start | bytes 1179656 | tf_op jit(solution)/shard_map/ppermute | solution.py:87
  12.0 12.0 %collective-permute-start.1 = (bf16[96,2048]{1,0:T(8,128)(2,1)S(1)}, bf16[96,2048]{1,0:T(8,128)(2,1)S(1)}, u32[]{:S(2)}, u32[]{:S(2)}) collective-permute-start(bf16[96,2048]{1,0:T(8,128)(2,1)S(1)} %fusion.14), channel_id=1, source_target_pairs={{0,16},{2,18},{4,20},{6,22},{8,24},{10,26},{12,28},{14,30},{16,0},... | collective-permute-start | bytes 1179656 | tf_op jit(solution)/shard_map/ppermute | solution.py:87
  13.4 17.3 %collective-permute-start.2 = (bf16[96,2048]{1,0:T(8,128)(2,1)S(1)}, bf16[96,2048]{1,0:T(8,128)(2,1)S(1)}, u32[]{:S(2)}, u32[]{:S(2)}) collective-permute-start(bf16[96,2048]{1,0:T(8,128)(2,1)S(1)} %fusion.14), channel_id=1, source_target_pairs={{0,18},{2,16},{4,22},{6,20},{8,26},{10,24},{12,30},{14,28},{16,2},... | collective-permute-start | bytes 1179656 | tf_op jit(solution)/shard_map/ppermute | solution.py:87
  32.2 99.1 %all-gather.7.cloned.1.call-start = ((), (), s32[]{:S(2)}) async-start(), calls=%async_computation.1 | async-start | bytes 5242880 | tf_op jit(solution)/shard_map/all_gather | solution.py:108
  35.1 12.9 %collective-permute-start.3 = (bf16[256,1024]{0,1:T(8,128)(2,1)S(1)}, bf16[256,1024]{0,1:T(8,128)(2,1)S(1)}, u32[]{:S(2)}, u32[]{:S(2)}) collective-permute-start(bf16[256,1024]{0,1:T(8,128)(2,1)S(1)} %pad_maximum_fusion.7), channel_id=1, source_target_pairs={{0,2},{2,0},{4,6},{6,4},{8,10},{10,8},{12,14},{14,12},{16,18},{18,... | collective-permute-start | bytes 1572872 | tf_op jit(solution)/shard_map/ppermute | solution.py:87
  49.3 171.5 %all-gather.11.cloned.1.call-start = ((), (), s32[]{:S(2)}) async-start(), calls=%async_computation.3 | async-start | bytes 5898240 | tf_op jit(solution)/shard_map/all_gather | solution.py:108
  50.8 5.3 %copy-start.4 = (f32[4]{0:T(128)S(1)}, f32[4]{0:T(128)}, u32[]{:S(2)}) copy-start(f32[4]{0:T(128)} %param.28) | copy-start | bytes 52
  52.3 13.4 %collective-permute-start.11 = (bf16[256,1152]{0,1:T(8,128)(2,1)S(1)}, bf16[256,1152]{0,1:T(8,128)(2,1)S(1)}, u32[]{:S(2)}, u32[]{:S(2)}) collective-permute-start(bf16[256,1152]{0,1:T(8,128)(2,1)S(1)} %pad_maximum_fusion.5), channel_id=1, source_target_pairs={{0,2},{2,0},{4,6},{6,4},{8,10},{10,8},{12,14},{14,12},{16,18},{18,... | collective-permute-start | bytes 1769480 | tf_op jit(solution)/shard_map/ppermute | solution.py:87
  67.1 165.6 %all-gather.9.cloned.1.call-start = ((), (), s32[]{:S(2)}) async-start(), calls=%async_computation.2 | async-start | bytes 4718592 | tf_op jit(solution)/shard_map/all_gather | solution.py:112
  137.2 0.8 copy-start.2
  141.6 3.8 %collective-permute-start.4 = (bf16[4,96,2048]{2,1,0:T(8,128)(2,1)}, bf16[4,96,2048]{2,1,0:T(8,128)(2,1)}, u32[]{:S(2)}, u32[]{:S(2)}) collective-permute-start(bf16[4,96,2048]{2,1,0:T(8,128)(2,1)} %constant_dynamic-slice_fusion.5), channel_id=1, source_target_pairs={{0,1},{1,0},{2,3},{3,2},{4,5},{5,4},{6,7},{7,6},{8,9},{9,8},{10,11... | collective-permute-start | bytes 4718600 | tf_op jit(solution)/shard_map/ppermute | solution.py:120
  147.4 20.9 %copy-start = (bf16[1,96,2048]{2,1,0:T(8,128)(2,1)S(1)}, bf16[1,96,2048]{2,1,0:T(8,128)(2,1)}, u32[]{:S(2)}) copy-start(bf16[1,96,2048]{2,1,0:T(8,128)(2,1)} %param.18) | copy-start | bytes 1179652
  147.5 21.3 %copy-start.1 = (f32[2048]{0:T(1024)S(1)}, f32[2048]{0:T(1024)}, u32[]{:S(2)}) copy-start(f32[2048]{0:T(1024)} %param.29) | copy-start | bytes 24580
  147.5 11.2 %collective-permute-start.5 = (bf16[96,2048]{1,0:T(8,128)(2,1)S(1)}, bf16[96,2048]{1,0:T(8,128)(2,1)S(1)}, u32[]{:S(2)}, u32[]{:S(2)}) collective-permute-start(bf16[96,2048]{1,0:T(8,128)(2,1)S(1)} %get-tuple-element.17), channel_id=1, source_target_pairs={{0,2},{2,0},{4,6},{6,4},{8,10},{10,8},{12,14},{14,12},{16,18},{18,... | collective-permute-start | bytes 1179656 | tf_op jit(solution)/shard_map/ppermute | solution.py:87
  149.1 12.0 %collective-permute-start.6 = (bf16[96,2048]{1,0:T(8,128)(2,1)S(1)}, bf16[96,2048]{1,0:T(8,128)(2,1)S(1)}, u32[]{:S(2)}, u32[]{:S(2)}) collective-permute-start(bf16[96,2048]{1,0:T(8,128)(2,1)S(1)} %get-tuple-element.19), channel_id=1, source_target_pairs={{0,16},{2,18},{4,20},{6,22},{8,24},{10,26},{12,28},{14,30},{16,0},... | collective-permute-start | bytes 1179656 | tf_op jit(solution)/shard_map/ppermute | solution.py:87
  150.6 17.8 %collective-permute-start.7 = (bf16[96,2048]{1,0:T(8,128)(2,1)S(1)}, bf16[96,2048]{1,0:T(8,128)(2,1)S(1)}, u32[]{:S(2)}, u32[]{:S(2)}) collective-permute-start(bf16[96,2048]{1,0:T(8,128)(2,1)S(1)} %get-tuple-element.18), channel_id=1, source_target_pairs={{0,18},{2,16},{4,22},{6,20},{8,26},{10,24},{12,30},{14,28},{16,2},... | collective-permute-start | bytes 1179656 | tf_op jit(solution)/shard_map/ppermute | solution.py:87
  169.0 11.1 %collective-permute-start.8 = (bf16[96,2048]{1,0:T(8,128)(2,1)S(1)}, bf16[96,2048]{1,0:T(8,128)(2,1)S(1)}, u32[]{:S(2)}, u32[]{:S(2)}) collective-permute-start(bf16[96,2048]{1,0:T(8,128)(2,1)S(1)} %fusion.20), channel_id=1, source_target_pairs={{0,2},{2,0},{4,6},{6,4},{8,10},{10,8},{12,14},{14,12},{16,18},{18,... | collective-permute-start | bytes 1179656 | tf_op jit(solution)/shard_map/ppermute | solution.py:87
  170.6 12.0 %collective-permute-start.9 = (bf16[96,2048]{1,0:T(8,128)(2,1)S(1)}, bf16[96,2048]{1,0:T(8,128)(2,1)S(1)}, u32[]{:S(2)}, u32[]{:S(2)}) collective-permute-start(bf16[96,2048]{1,0:T(8,128)(2,1)S(1)} %fusion.20), channel_id=1, source_target_pairs={{0,16},{2,18},{4,20},{6,22},{8,24},{10,26},{12,28},{14,30},{16,0},... | collective-permute-start | bytes 1179656 | tf_op jit(solution)/shard_map/ppermute | solution.py:87
  172.0 16.7 %collective-permute-start.10 = (bf16[96,2048]{1,0:T(8,128)(2,1)S(1)}, bf16[96,2048]{1,0:T(8,128)(2,1)S(1)}, u32[]{:S(2)}, u32[]{:S(2)}) collective-permute-start(bf16[96,2048]{1,0:T(8,128)(2,1)S(1)} %fusion.20), channel_id=1, source_target_pairs={{0,18},{2,16},{4,22},{6,20},{8,26},{10,24},{12,30},{14,28},{16,2},... | collective-permute-start | bytes 1179656 | tf_op jit(solution)/shard_map/ppermute | solution.py:87
  232.8 5.5 %copy-start.3 = (f32[2048]{0:T(1024)S(1)}, f32[2048]{0:T(1024)}, u32[]{:S(2)}) copy-start(f32[2048]{0:T(1024)} %param.35) | copy-start | bytes 24580
  241.7 3.5 %collective-permute-start.12 = (bf16[4,96,2048]{2,1,0:T(8,128)(2,1)S(1)}, bf16[4,96,2048]{2,1,0:T(8,128)(2,1)S(1)}, u32[]{:S(2)}, u32[]{:S(2)}) collective-permute-start(bf16[4,96,2048]{2,1,0:T(8,128)(2,1)S(1)} %constant_dynamic-slice_fusion), channel_id=1, source_target_pairs={{0,1},{1,0},{2,3},{3,2},{4,5},{5,4},{6,7},{7,6},{8,9},{9,8},{10,11... | collective-permute-start | bytes 4718600 | tf_op jit(solution)/shard_map/ppermute | solution.py:120
  246.0 11.4 %collective-permute-start.13 = (bf16[96,2048]{1,0:T(8,128)(2,1)S(1)}, bf16[96,2048]{1,0:T(8,128)(2,1)S(1)}, u32[]{:S(2)}, u32[]{:S(2)}) collective-permute-start(bf16[96,2048]{1,0:T(8,128)(2,1)S(1)} %get-tuple-element.14), channel_id=1, source_target_pairs={{0,2},{2,0},{4,6},{6,4},{8,10},{10,8},{12,14},{14,12},{16,18},{18,... | collective-permute-start | bytes 1179656 | tf_op jit(solution)/shard_map/ppermute | solution.py:87
  247.8 12.0 %collective-permute-start.14 = (bf16[96,2048]{1,0:T(8,128)(2,1)S(1)}, bf16[96,2048]{1,0:T(8,128)(2,1)S(1)}, u32[]{:S(2)}, u32[]{:S(2)}) collective-permute-start(bf16[96,2048]{1,0:T(8,128)(2,1)S(1)} %get-tuple-element.16), channel_id=1, source_target_pairs={{0,16},{2,18},{4,20},{6,22},{8,24},{10,26},{12,28},{14,30},{16,0},... | collective-permute-start | bytes 1179656 | tf_op jit(solution)/shard_map/ppermute | solution.py:87
  249.3 17.8 %collective-permute-start.15 = (bf16[96,2048]{1,0:T(8,128)(2,1)S(1)}, bf16[96,2048]{1,0:T(8,128)(2,1)S(1)}, u32[]{:S(2)}, u32[]{:S(2)}) collective-permute-start(bf16[96,2048]{1,0:T(8,128)(2,1)S(1)} %get-tuple-element.15), channel_id=1, source_target_pairs={{0,18},{2,16},{4,22},{6,20},{8,26},{10,24},{12,30},{14,28},{16,2},... | collective-permute-start | bytes 1179656 | tf_op jit(solution)/shard_map/ppermute | solution.py:87
Sparse Core Ops, SparseCore 0:
  32.3 13.5 all-gather.4
  49.4 81.8 all-gather.6
  132.9 87.8 all-gather.10
  222.2 10.5 all-gather.8
